TPU v7x, 128 devices: a whole 4x4x4 slice. The times are simulated.
128 devices in a mesh: sp: 16 (over z, x), tp: 8 (over y, core).
Axes of the slice: x: 4, y: 4, z: 4, core: 2. Of those that a mesh axis runs over, the one named last changes fastest.
Arguments:
- query_small: bfloat16 [12288, 1024], P('sp', 'tp'), may hold values from -6 to 6
- key_small: bfloat16 [12288, 1024], P('sp', 'tp'), may hold values from -6 to 6
- value_small: bfloat16 [12288, 1024], P('sp', 'tp'), may hold values from -6 to 6
- gates_small: float32 [12288, 16], P('sp', 'tp'), as said below
- query_large: bfloat16 [12288, 1024], P('sp', 'tp'), may hold values from -6 to 6
- key_large: bfloat16 [12288, 1024], P('sp', 'tp'), may hold values from -6 to 6
- value_large: bfloat16 [12288, 1024], P('sp', 'tp'), may hold values from -6 to 6
- gates_large: float32 [12288, 8], P('sp', 'tp'), as said below
- residual: bfloat16 [12288, 2048], P(('sp', 'tp')), may hold values from -6 to 6
- mixer_small: bfloat16 [1024, 2048], P('tp'), may hold values from -1 to 1
- mixer_large: bfloat16 [1024, 2048], P('tp'), may hold values from -1 to 1
- mix_gain: float32 [2048], replicated, may hold values from 0.1 to 1.9
- value_weight: bfloat16 [2048, 5632], P('sp', 'tp'), may hold values from -0.125 to 0.125
- gate_weight: bfloat16 [2048, 5632], P('sp', 'tp'), may hold values from -0.125 to 0.125
- value_taps: float32 [3, 5632], P(None, 'tp'), may hold values from -3 to 3
- gate_taps: float32 [3, 5632], P(None, 'tp'), may hold values from -3 to 3
- down_weight: bfloat16 [5632, 2048], P('tp', 'sp'), may hold values from -0.078125 to 0.078125
- final_gain: float32 [2048], replicated, may hold values from 0.1 to 1.9
Outputs:
- layer_out: bfloat16 [12288, 2048], P(('sp', 'tp'))
Inputs may be any that keep to these rules, and one draw needn't show every extreme that they name: `gates_small`: each column never rises from one position to the next, and its first entry is negative. `gates_large`: each column never rises from one position to the next, and its first entry is negative.
All inputs are finite; a program needn't handle non-finite values.
Results may differ from a plain program's by a relative error of at most 0.018.
Values may be sent and summed in bfloat16 or wider, within the bound.
No kernel may reach another device: no remote copies, remote signals or barrier semaphores. Data moves between devices by JAX's collectives and lax.ppermute only.
A program may use at most 128 MiB of HBM per device.

v0:
```python
import math

import jax
import jax.numpy as jnp
from jax import lax
from jax.sharding import Mesh
from jax.sharding import PartitionSpec as P

DS = 64
DL = 128
TP = ("tp_0", "tp_1")
SP_TP = ("sp", "tp_0", "tp_1")


residual_scale = 2.0**0.5
epsilon = 1e-05


def gather_turned(arrays, axis, dims):
    turned = [jnp.moveaxis(a, dim, 0) for a, dim in zip(arrays, dims)]
    widths = [t[0].size for t in turned]
    both = jnp.concatenate([t.reshape(-1, w) for t, w in zip(turned, widths)], axis=1)
    out = lax.all_gather(both, axis, axis=0, tiled=True)
    pieces = jnp.split(out, [sum(widths[:k]) for k in range(1, len(widths))], axis=1)
    return tuple(
        (
            jnp.moveaxis(b.reshape(-1, *t.shape[1:]), 0, dim)
            for b, t, dim in zip(pieces, turned, dims)
        )
    )


def sent_together(arrays, axis, dim, along):
    both = jnp.concatenate(arrays, axis=along)
    out, at, finished = (lax.all_gather(both, axis, axis=dim, tiled=True), 0, [])
    for a in arrays:
        finished.append(lax.slice_in_dim(out, at, at + a.shape[along], axis=along))
        at += a.shape[along]
    return tuple(finished)


def split_up(array, dim, devices):
    shape = array.shape
    pieces = array.reshape(*shape[:dim], devices, shape[dim] // devices, *shape[dim + 1 :])
    return jnp.moveaxis(pieces, dim, 0)


def laid_out(pieces, dim):
    shape = list(pieces.shape[1:])
    shape[dim] *= pieces.shape[0]
    return jnp.moveaxis(pieces, 0, dim).reshape(shape)


def moved_by_axis(pieces, axes, turns):
    shape = [lax.axis_size(a) for a in axes]
    pieces = pieces.reshape(*shape, *pieces.shape[1:])
    for k in turns:
        pieces = lax.all_to_all(pieces, axes[k], split_axis=k, concat_axis=k, tiled=True)
    return pieces.reshape(-1, *pieces.shape[len(axes) :])


def stepwise_exchange(array, axes, turns, split_dim, concat_dim):
    pieces = split_up(array, split_dim, lax.axis_size(axes))
    return laid_out(moved_by_axis(pieces, axes, turns), concat_dim)


def passed_along(value, axis, steps):
    count = lax.axis_size(axis)
    first, last = (max(0, -steps), min(count, count - steps))
    return lax.ppermute(value, axis, [(source, source + steps) for source in range(first, last)])


def norm_rows(values, gain):
    center = jnp.mean(values, axis=-1, keepdims=True)
    spread = jnp.mean(jnp.square(values - center), axis=-1, keepdims=True)
    return (values - center) * lax.rsqrt(spread + epsilon) * gain


def attend_block(
    running,
    queries,
    query_gates,
    key_rows,
    value_rows,
    key_gates,
    token_positions,
    key_first,
    head_dim,
):
    running_peak, weight_sum, weighted = running
    heads_here = query_gates.shape[1]
    span_rows = key_rows.shape[0]
    query_heads = queries.reshape(queries.shape[0], heads_here, head_dim)
    key_heads = key_rows.reshape(span_rows, heads_here, head_dim)
    value_heads = value_rows.reshape(span_rows, heads_here, head_dim)
    scores = jnp.einsum(
        "qhd,khd->hqk", query_heads, key_heads, preferred_element_type=jnp.float32
    ) * head_dim ** (-0.5)
    scores = scores + query_gates.T[:, :, None] - key_gates.T[:, None, :]
    key_positions = key_first + jnp.arange(span_rows)
    allowed = token_positions[:, None] >= key_positions[None, :]
    scores = jnp.where(allowed[None], scores, -1e30)
    new_peak = jnp.maximum(running_peak, jnp.max(scores, axis=-1))
    factor = jnp.exp(running_peak - new_peak)
    weights = jnp.where(allowed[None], jnp.exp(scores - new_peak[:, :, None]), 0.0)
    weight_sum = weight_sum * factor + jnp.sum(weights, axis=-1)
    update = jnp.einsum(
        "hqk,khd->qhd",
        weights.astype(jnp.bfloat16),
        value_heads,
        preferred_element_type=jnp.float32,
    )
    weighted = weighted * factor.T[:, :, None] + update
    return (new_peak, weight_sum, weighted)


def per_device(
    query_small,
    key_small,
    value_small,
    gates_small,
    query_large,
    key_large,
    value_large,
    gates_large,
    residual,
    mixer_small,
    mixer_large,
    mix_gain,
    value_weight,
    gate_weight,
    value_taps,
    gate_taps,
    down_weight,
    final_gain,
):
    shard_rows = query_small.shape[0]
    first_row = lax.axis_index("sp") * shard_rows
    token_positions = first_row + jnp.arange(shard_rows)
    last_position = first_row + shard_rows - 1
    whole_value, whole_gate, whole_down = gather_turned(
        (value_weight, gate_weight, down_weight), "sp", (0, 0, 1)
    )
    every_gate = (
        lax.all_gather(gates_small, "sp", axis=0, tiled=True),
        lax.all_gather(gates_large, "sp", axis=0, tiled=True),
    )
    heads_small = gates_small.shape[1]
    heads_large = gates_large.shape[1]

    def fresh(heads_here, head_dim):
        return (
            jnp.full((heads_here, shard_rows), -1e30, jnp.float32),
            jnp.zeros((heads_here, shard_rows), jnp.float32),
            jnp.zeros((shard_rows, heads_here, head_dim), jnp.float32),
        )

    pieces = sent_together((key_small, value_small, key_large, value_large), "sp", 0, 1)
    span_total = pieces[0].shape[0]
    block_rows = shard_rows * math.gcd(span_total // shard_rows, max(1, 1024 // shard_rows))

    def one_block(block_index, current):
        offset = block_index * block_rows
        sliced = [lax.dynamic_slice_in_dim(member, offset, block_rows, 0) for member in pieces]
        gate_small = lax.dynamic_slice_in_dim(every_gate[0], offset, block_rows, 0)
        gate_large = lax.dynamic_slice_in_dim(every_gate[1], offset, block_rows, 0)

        def update(previous):
            return (
                attend_block(
                    previous[0],
                    query_small,
                    gates_small,
                    sliced[0],
                    sliced[1],
                    gate_small,
                    token_positions,
                    offset,
                    DS,
                ),
                attend_block(
                    previous[1],
                    query_large,
                    gates_large,
                    sliced[2],
                    sliced[3],
                    gate_large,
                    token_positions,
                    offset,
                    DL,
                ),
            )

        def unchanged(previous):
            return previous

        return lax.cond(offset <= last_position, update, unchanged, current)

    block_count = span_total // block_rows
    small_state, large_state = lax.fori_loop(
        0, block_count, one_block, (fresh(heads_small, DS), fresh(heads_large, DL))
    )
    small_out = (
        (small_state[2] / small_state[1].T[:, :, None])
        .reshape(shard_rows, heads_small * DS)
        .astype(jnp.bfloat16)
    )
    large_out = (
        (large_state[2] / large_state[1].T[:, :, None])
        .reshape(shard_rows, heads_large * DL)
        .astype(jnp.bfloat16)
    )
    tensor_parts = lax.axis_size(TP)
    own_rows = shard_rows // tensor_parts
    joined = jnp.concatenate([small_out, large_out], axis=1)
    arrived = stepwise_exchange(joined, TP, (1, 0), 0, 1)
    layout = arrived.reshape(own_rows, tensor_parts, joined.shape[1])
    small_width = small_out.shape[1]
    all_small = layout[:, :, :small_width].reshape(own_rows, tensor_parts * small_width)
    all_large = layout[:, :, small_width:].reshape(own_rows, tensor_parts * large_out.shape[1])
    add_pieces = sent_together((mixer_small, mixer_large), TP, 0, 1)
    mix = jnp.dot(all_small, add_pieces[0], preferred_element_type=jnp.float32) + jnp.dot(
        all_large, add_pieces[1], preferred_element_type=jnp.float32
    )
    mixed = norm_rows(residual_scale * residual.astype(jnp.float32) + mix, mix_gain).astype(
        jnp.bfloat16
    )
    block_input = lax.all_gather(mixed, TP, axis=0, tiled=True)
    up_value = jnp.dot(block_input, whole_value, preferred_element_type=jnp.float32)
    up_gate = jnp.dot(block_input, whole_gate, preferred_element_type=jnp.float32)
    up_value = up_value.astype(jnp.bfloat16)
    up_gate = up_gate.astype(jnp.bfloat16)
    hidden_width = up_value.shape[1]
    trailing = jnp.concatenate([up_value[-2:], up_gate[-2:]], axis=1)
    earlier = passed_along(trailing, "sp", 1)
    padded_value = jnp.concatenate([earlier[:, :hidden_width], up_value], axis=0).astype(
        jnp.float32
    )
    padded_gate = jnp.concatenate([earlier[:, hidden_width:], up_gate], axis=0).astype(jnp.float32)
    filt_value = (
        value_taps[0] * padded_value[:-2]
        + value_taps[1] * padded_value[1:-1]
        + value_taps[2] * padded_value[2:]
    )
    filt_gate = (
        gate_taps[0] * padded_gate[:-2]
        + gate_taps[1] * padded_gate[1:-1]
        + gate_taps[2] * padded_gate[2:]
    )
    hidden = (jax.nn.silu(filt_gate) * filt_value).astype(jnp.bfloat16)
    ffn_terms = jnp.dot(hidden, whole_down, preferred_element_type=jnp.float32)
    ffn = lax.psum_scatter(
        ffn_terms.astype(jnp.bfloat16), TP, scatter_dimension=0, tiled=True
    ).astype(jnp.float32)
    return norm_rows(residual_scale * mixed.astype(jnp.float32) + ffn, final_gain).astype(
        jnp.bfloat16
    )


def solution(mesh):
    split = Mesh(mesh.devices.reshape(mesh.shape["sp"], 4, 2), ("sp", "tp_0", "tp_1"))
    placed = (
        P("sp", TP),
        P("sp", TP),
        P("sp", TP),
        P("sp", TP),
        P("sp", TP),
        P("sp", TP),
        P("sp", TP),
        P("sp", TP),
        P(SP_TP, None),
        P(TP, None),
        P(TP, None),
        P(),
        P("sp", TP),
        P("sp", TP),
        P(None, TP),
        P(None, TP),
        P(TP, "sp"),
        P(),
    )
    return jax.shard_map(
        per_device, mesh=split, in_specs=placed, out_specs=P(SP_TP, None), check_vma=False
    )
```

profile of v0, /device:TPU:0, one launch (start us, length us, event | category | flops | bytes accessed | tf_op | source)
XLA Modules:
  0.0 428.5 jit_solution(15232635295806895450)
XLA Ops:
  6.5 2.3 pad_maximum_fusion.1
  8.9 0.0 all-gather.5.cloned.1.call-update
  8.9 0.0 copy-start.4
  8.9 0.0 copy-start.9
  8.9 0.0 copy-start.3
  9.0 0.0 all-gather.7.cloned.1.call-start
  9.0 1.0 pad_maximum_fusion
  10.0 0.0 all-gather.7.cloned.1.call-update
  10.1 0.0 all-gather.11.cloned.1.call-start
  10.1 0.9 pad_maximum_fusion.2
  11.0 0.0 all-gather.11.cloned.1.call-update
  11.1 0.0 all-gather.9.cloned.1.call-start
  11.1 0.1 copy.44
  11.3 25.3 %all_gather.20 = f32[12288,1]{0,1:T(1,128)S(1)} all-gather(f32[768,1]{0,1:T(1,128)S(1)} %copy-done.9), channel_id=1, replica_groups=mesh['sp'=16,'tp_0'=4,'tp_1'=2] {'sp'}, dimensions={0}, use_global_device_ids=true | all-gather | bytes 52224 | tf_op jit(solution)/shard_map/all_gather | solution.py:146
  36.5 23.9 %all_gather.19 = f32[12288,2]{0,1:T(2,128)S(1)} all-gather(f32[768,2]{0,1:T(2,128)S(1)} %copy-done.3), channel_id=1, replica_groups=mesh['sp'=16,'tp_0'=4,'tp_1'=2] {'sp'}, dimensions={0}, use_global_device_ids=true | all-gather | bytes 104448 | tf_op jit(solution)/shard_map/all_gather | solution.py:145
  60.4 42.2 %all-gather.5.cloned.1.call-done = bf16[12288,512]{1,0:T(8,128)(2,1)} async-done(((bf16[768,512]{1,0:T(8,128)(2,1)}), bf16[12288,512]{1,0:T(8,128)(2,1)}) %all-gather.5.cloned.1.call-update) | async-done | bytes 12582928 | tf_op jit(solution)/shard_map/all_gather | solution.py:35
  102.6 8.7 %fusion.66 = (bf16[12288,128]{1,0:T(8,128)(2,1)}, bf16[12288,128]{1,0:T(8,128)(2,1)}, bf16[12288,128]{1,0:T(8,128)(2,1)S(1)}, bf16[12288,128]{1,0:T(8,128)(2,1)}) fusion(bf16[12288,512]{1,0:T(8,128)(2,1)} %all-gather.5.cloned.1.call-done), kind=kLoop, calls=%fused_computation.99 | loop fusion | bytes 25165824 | tf_op jit(solution)/shard_map/slice | solution.py:37
  111.3 4.8 %copy.43 = bf16[12288,128]{0,1:T(8,128)(2,1)} copy(bf16[12288,128]{1,0:T(8,128)(2,1)} %get-tuple-element.740) | data formatting | bytes 6291456
  116.1 2.9 copy.45
  119.1 12.2 %while.24 = (s32[]{:T(128)}, f32[2,768]{1,0:T(2,128)S(1)}, f32[2,768]{1,0:T(2,128)S(1)}, f32[768,2,64]{0,2,1:T(8,128)S(1)}, f32[1,768]{1,0:T(1,128)S(1)}, /*inde...) while((s32[]{:T(128)}, f32[2,768]{1,0:T(2,128)S(1)}, ...), condition=%wide.region_7.8_spmd.clone, body=%wide.region_0.7_spmd.clone.sunk | while | flops 640360704 | bytes 27399704 | solution.py:200
  119.1 11.3 %conditional.3 = ((f32[2,768]{1,0:T(2,128)S(1)}, f32[2,768]{1,0:T(2,128)S(1)}, f32[768,2,64]{0,2,1:T(8,128)S(1)}, f32[1,768]{1,0:T(1,128)S(1)}, f32[1,768]{1,0:T(1,128)S(1)}, /*index=5*/f32[768,1,128]{0,2,1:T(8,128)S(1)})) conditional(s32[]{:T(128)} %convert_element_type.124, (f32[2,768]{1,0:T(2,128)S(1)}, f32[2,768]{1,0:T(2,128)S(1)}, ...), branch_computations={%region_1.0_spmd, %region_2.6_spmd} | conditional | flops 640360704 | bytes 27396218 | solution.py:197
  119.2 1.7 fusion.8
  120.9 1.9 fusion.17
  122.9 0.8 fusion.10
  123.7 0.4 broadcast_compare_fusion
  124.2 1.1 constant_dynamic-slice_fusion
  125.2 1.5 fusion.4
  126.7 2.0 fusion.14
  128.7 1.7 fusion.3
  131.4 0.3 convert_element_type.69
  131.7 0.2 copy.46
  131.9 0.2 divide_convert_fusion
  132.0 0.2 copy.47
  132.2 0.8 pad_maximum_fusion.3
  133.0 0.5 copy.48
  133.6 4.0 all_to_all.10
  137.7 17.6 %all_to_all.11 = bf16[4,2,96,256]{3,2,1,0:T(8,128)(2,1)S(1)} all-to-all(bf16[4,2,96,256]{3,2,1,0:T(8,128)(2,1)S(1)} %copy.49), channel_id=1, replica_groups=mesh['sp'=16,'tp_0'=4,'tp_1'=2] {'tp_0'}, dimensions={0} | all-to-all | bytes 786432 | tf_op jit(solution)/shard_map/all_to_all | solution.py:58
  155.2 0.2 copy.65
  155.5 2.4 all-gather.7.cloned.1.call-done
  157.8 3.0 fusion.32
  160.9 0.0 copy-start.8
  160.9 3.2 fusion.69
  164.1 0.2 multiply_reduce_fusion.1
  164.4 0.9 multiply_convert_fusion.1
  165.3 0.0 all-gather.9.cloned.1.call-update
  165.3 0.0 reduce-scatter.2.cloned.1.call-start
  165.4 69.2 %all-gather.11.cloned.1.call-done = bf16[2048,2112]{0,1:T(8,128)(2,1)} async-done(((bf16[128,2112]{0,1:T(8,128)(2,1)}), bf16[2048,2112]{0,1:T(8,128)(2,1)}) %all-gather.11.cloned.1.call-update) | async-done | bytes 8650768 | tf_op jit(solution)/shard_map/all_gather | solution.py:23
  234.6 118.0 %all-gather.9.cloned.1.call-done = bf16[768,2048]{1,0:T(8,128)(2,1)} async-done(((bf16[96,2048]{1,0:T(8,128)(2,1)}), bf16[768,2048]{1,0:T(8,128)(2,1)}) %all-gather.9.cloned.1.call-update) | async-done | bytes 3145744 | tf_op jit(solution)/shard_map/all_gather | solution.py:228
  352.5 5.3 %fusion.53 = bf16[768,704]{0,1:T(8,128)(2,1)S(1)} fusion(bf16[768,2048]{1,0:T(8,128)(2,1)} %all-gather.9.cloned.1.call-done, bf16[2048,2112]{0,1:T(8,128)(2,1)} %all-gather.11.cloned.1.call-done), kind=kOutput, calls=%fused_computation.66 | convolution fusion | flops 2215133184 | bytes 7110656 | tf_op jit(solution)/shard_map/dot_general | solution.py:229
  357.9 0.1 slice.104
  358.0 0.6 copy-done.14
  358.7 2.4 fusion.56
  361.1 0.1 slice.105
  361.2 0.1 pad_maximum_fusion.4
  361.3 3.6 collective-permute-start
  365.0 0.1 slice_reduce_fusion.2
  365.0 7.7 %collective-permute-done = bf16[2,1408]{0,1:T(8,128)(2,1)S(1)} collective-permute-done((bf16[2,1408]{0,1:T(8,128)(2,1)S(1)}, bf16[2,1408]{0,1:T(8,128)(2,1)S(1)}, u32[]{:S(2)}, u32[]{:S(2)}) %collective-permute-start) | collective-permute-done | bytes 5664 | tf_op jit(solution)/shard_map/ppermute | solution.py:70
  372.8 1.1 maximum_convert_fusion
  373.9 7.0 %convolution_convert_fusion = bf16[768,2048]{1,0:T(8,128)(2,1)} fusion(bf16[2048,2112]{0,1:T(8,128)(2,1)S(1)} %copy-done.13, f32[770,704]{0,1:T(8,128)S(1)} %get-tuple-element.748, f32[770,704]{0,1:T(8,128)S(1)} %get-tuple-element.747, f32[704]{0:T(1024)S(1)} %get-tuple-element.686, f32[704]{0:T(1024)S(1)} %get-tuple-element.687, ...), kind=kOutput, calls=%fused_computation.46 | convolution fusion | flops 2224816128 | bytes 19030016 | tf_op jit(solution)/shard_map/dot_general | solution.py:251
  380.8 0.0 reduce-scatter.2.cloned.1.call-update
  380.8 37.0 %reduce-scatter.2.cloned.1.call-done = bf16[96,2048]{1,0:T(8,128)(2,1)} async-done(((bf16[768,2048]{1,0:T(8,128)(2,1)}), bf16[96,2048]{1,0:T(8,128)(2,1)}) %reduce-scatter.2.cloned.1.call-update) | async-done | bytes 393232 | tf_op jit(solution)/shard_map/reduce_scatter | solution.py:252
  417.9 1.4 fusion.60
  419.3 1.4 multiply_reduce_fusion
  420.8 1.2 multiply_convert_fusion
  (84 shorter events, 0.7 us)
Async XLA Ops:
  6.5 2.5 copy-start.2
  6.5 2.5 copy-start.1
  6.5 96.1 %all-gather.5.cloned.1.call-start = ((), (), s32[]{:S(2)}) async-start(), calls=%async_computation.3 | async-start | bytes 13369344 | tf_op jit(solution)/shard_map/all_gather | solution.py:35
  8.9 1.2 copy-start.5
  8.9 1.2 copy-start.6
  8.9 1.2 copy-start.7
  8.9 2.2 copy-start.4
  8.9 2.4 copy-start.9
  8.9 27.6 %copy-start.3 = (f32[768,2]{0,1:T(2,128)S(1)}, f32[768,2]{0,1:T(2,128)}, u32[]{:S(2)}) copy-start(f32[768,2]{0,1:T(2,128)} %param.25) | copy-start | bytes 18436
  9.0 148.9 %all-gather.7.cloned.1.call-start = ((), (), s32[]{:S(2)}) async-start(), calls=%async_computation.4 | async-start | bytes 9437184 | tf_op jit(solution)/shard_map/all_gather | solution.py:35
  10.1 224.5 %all-gather.11.cloned.1.call-start = ((), (), s32[]{:S(2)}) async-start(), calls=%async_computation.6 | async-start | bytes 9191424 | tf_op jit(solution)/shard_map/all_gather | solution.py:23
  11.1 341.5 %all-gather.9.cloned.1.call-start = ((), (), s32[]{:S(2)}) async-start(), calls=%async_computation.5 | async-start | bytes 3538944 | tf_op jit(solution)/shard_map/all_gather | solution.py:228
  157.8 3.0 copy-start.15
  160.9 3.5 copy-start.8
  165.3 252.6 %reduce-scatter.2.cloned.1.call-start = ((), (), s32[]{:S(2)}) async-start(), calls=%async_computation.7 | async-start | bytes 3538944 | tf_op jit(solution)/shard_map/reduce_scatter | solution.py:252
  352.5 5.5 %copy-start.13 = (bf16[2048,2112]{0,1:T(8,128)(2,1)S(1)}, bf16[2048,2112]{0,1:T(8,128)(2,1)}, u32[]{:S(2)}) copy-start(bf16[2048,2112]{0,1:T(8,128)(2,1)} %all-gather.11.cloned.1.call-done) | copy-start | bytes 25952260
  352.5 6.1 %copy-start.14 = (bf16[768,2048]{1,0:T(8,128)(2,1)S(1)}, bf16[768,2048]{1,0:T(8,128)(2,1)}, u32[]{:S(2)}) copy-start(bf16[768,2048]{1,0:T(8,128)(2,1)} %all-gather.9.cloned.1.call-done) | copy-start | bytes 9437188
  358.7 6.3 %copy-start.11 = (f32[3,704]{1,0:T(4,128)S(1)}, f32[3,704]{1,0:T(4,128)}, u32[]{:S(2)}) copy-start(f32[3,704]{1,0:T(4,128)} %param.36) | copy-start | bytes 25348
  358.7 6.3 %copy-start.12 = (f32[3,704]{1,0:T(4,128)S(1)}, f32[3,704]{1,0:T(4,128)}, u32[]{:S(2)}) copy-start(f32[3,704]{1,0:T(4,128)} %param.37) | copy-start | bytes 25348
  361.3 11.4 %collective-permute-start = (bf16[2,1408]{0,1:T(8,128)(2,1)S(1)}, bf16[2,1408]{0,1:T(8,128)(2,1)S(1)}, u32[]{:S(2)}, u32[]{:S(2)}) collective-permute-start(bf16[2,1408]{0,1:T(8,128)(2,1)S(1)} %pad_maximum_fusion.4), channel_id=1, source_target_pairs={{0,8},{8,16},{16,24},{24,32},{32,40},{40,48},{48,56},{56,64},{64,7... | collective-permute-start | bytes 16904 | tf_op jit(solution)/shard_map/ppermute | solution.py:70
  380.8 39.9 %copy-start.10 = (f32[2048]{0:T(1024)S(1)}, f32[2048]{0:T(1024)}, u32[]{:S(2)}) copy-start(f32[2048]{0:T(1024)} %param.39) | copy-start | bytes 24580
  417.9 2.9 copy-start
Sparse Core Ops, SparseCore 0:
  9.5 93.1 all-gather.4
  104.4 53.4 all-gather.6
  160.0 74.5 all-gather.10
  236.1 116.3 all-gather.8
  381.0 36.8 reduce-scatter.1
where the time goes:
time: 430 us; the launch traced here: 428 us
  waiting for transfers between devices  277 us (64%)
  blocking collectives  70.8 us (16%)
  matrix products  28.1 us (7%)
  local copies, waits for them, and re-layouts  20.1 us (5%)
  other arithmetic  14.6 us (3%)
  between operations  13.5 us (3%)
    all_gather x1, waiting for transfers between devices, per_device(): block_input = lax.all_gather(mixed, TP, axis=0, tiled=True)  118 us
    all_gather x1, waiting for transfers between devices, gather_turned(): out = lax.all_gather(both, axis, axis=0, tiled=True)  69.2 us
    all_gather x2, waiting for transfers between devices, sent_together(): lax.all_gather(both, axis, axis=dim, tiled=True)  44.6 us
    reduce_scatter x1, waiting for transfers between devices, per_device(): lax.psum_scatter(ffn_terms.astype(jnp.bfloat16), TP, scatter_dimension=0,...  37 us
    all_gather x1, blocking collectives, per_device(): lax.all_gather(gates_large, 'sp', axis=0, tiled=True)  25.3 us
    all_gather x1, blocking collectives, per_device(): lax.all_gather(gates_small, 'sp', axis=0, tiled=True)  23.9 us
    all_to_all x2, blocking collectives, moved_by_axis(): lax.all_to_all(pieces, axes[k], split_axis=k, concat_axis=k, tiled=True)  21.6 us
    slice x1, local copies, waits for them, and re-layouts, sent_together(): finished.append(lax.slice_in_dim(out, at, at + a.shape[along], axis=along))  8.66 us
  transfers between devices with their start and end apart: 6, of which 6 were waited for; matrix products, arithmetic and copies ran while one was open for 9% of the time, Pallas kernels for 0%

commit v1 on v0

v1 whole, which is shorter than its diff:
```python
import math

import jax
import jax.numpy as jnp
from jax import lax
from jax.experimental import pallas as pl
from jax.experimental.pallas import tpu as pltpu
from jax.sharding import Mesh
from jax.sharding import PartitionSpec as P

DS = 64
DL = 128
TP = ("tp_0", "tp_1")
SP_TP = ("sp", "tp_0", "tp_1")
bf16 = jnp.bfloat16
f32 = jnp.float32


residual_scale = 2.0**0.5
epsilon = 1e-05


def gather_turned(arrays, axis, dims):
    turned = [jnp.moveaxis(a, dim, 0) for a, dim in zip(arrays, dims)]
    widths = [t[0].size for t in turned]
    both = jnp.concatenate([t.reshape(-1, w) for t, w in zip(turned, widths)], axis=1)
    out = lax.all_gather(both, axis, axis=0, tiled=True)
    pieces = jnp.split(out, [sum(widths[:k]) for k in range(1, len(widths))], axis=1)
    return tuple(
        (
            jnp.moveaxis(b.reshape(-1, *t.shape[1:]), 0, dim)
            for b, t, dim in zip(pieces, turned, dims)
        )
    )


def sent_together(arrays, axis, dim, along):
    both = jnp.concatenate(arrays, axis=along)
    out, at, finished = (lax.all_gather(both, axis, axis=dim, tiled=True), 0, [])
    for a in arrays:
        finished.append(lax.slice_in_dim(out, at, at + a.shape[along], axis=along))
        at += a.shape[along]
    return tuple(finished)


def passed_along(value, axis, steps):
    count = lax.axis_size(axis)
    first, last = (max(0, -steps), min(count, count - steps))
    return lax.ppermute(value, axis, [(source, source + steps) for source in range(first, last)])


def norm_rows(values, gain):
    center = jnp.mean(values, axis=-1, keepdims=True)
    spread = jnp.mean(jnp.square(values - center), axis=-1, keepdims=True)
    return (values - center) * lax.rsqrt(spread + epsilon) * gain


def attend(q, kv, gates, rank, heads, base):
    rows = q.shape[0]
    width = q.shape[1]
    d = width // heads
    chunk = 256
    chunks = rows // chunk
    ext = d + 16
    deep = width if heads == 2 else 2 * width
    root = d ** 0.5
    rate = math.log2(math.e) / root
    units = [(h, c) for h in range(heads) for c in range(chunks)]

    def body(rank_ref, q_ref, kv_ref, g_ref, o_ref, qa, ka, va, acc, peak, first):
        me = rank_ref[0]
        lane = lax.broadcasted_iota(jnp.int32, (rows, width), 1)
        for h in range(heads):
            if heads == 2:
                mine = (lane < d) if h == 0 else (lane >= d)
                at = d if h == 0 else 0
                one = ((lane >= at) & (lane < at + 3)).astype(f32)
                qa[h] = jnp.where(mine, q_ref[...].astype(f32), one).astype(bf16)
            else:
                qa[h, :, :width] = q_ref[...]
                qa[h, :, width:] = (lane < 3).astype(f32).astype(bf16)
            va[0, h, d:] = jnp.ones((16, rows), bf16)
            va[1, h, d:] = jnp.ones((16, rows), bf16)
        acc[...] = jnp.zeros(acc.shape, f32)
        peak[...] = jnp.full(peak.shape, -1e30, f32)
        start = g_ref[me][:, 0:1]

        def prepare(j, slot):
            at = pl.multiple_of(j * rows, rows)
            k = kv_ref[pl.ds(at, rows), :width]
            vt = kv_ref[pl.ds(at, rows), width:].T
            bias = jnp.maximum((start - g_ref[j]) * root, -1e30)
            hi = bias.astype(bf16).astype(f32)
            mid = (bias - hi).astype(bf16).astype(f32)
            low = bias - hi - mid
            zero = jnp.zeros((8, rows), f32)
            row = lax.broadcasted_iota(jnp.int32, (8, rows), 0)
            parts = []
            for h in range(heads):
                pick = lambda a: jnp.broadcast_to(a[base + h : base + h + 1], (8, rows))
                parts.append(jnp.where(row == 0, pick(hi), jnp.where(row == 1, pick(mid), jnp.where(row == 2, pick(low), zero))))
            if heads == 2:
                pad = jnp.zeros((d - 8, rows), f32)
                gt = jnp.concatenate([parts[1], pad, parts[0], pad], axis=0)
            else:
                gt = jnp.concatenate([parts[0], jnp.zeros((width - 8, rows), f32)], axis=0)
            gc = gt.astype(bf16).T
            for h in range(heads):
                if heads == 2:
                    mine = (lane < d) if h == 0 else (lane >= d)
                    ka[slot, h] = jnp.where(mine, k, gc)
                else:
                    ka[slot, h, :, :width] = k
                    ka[slot, h, :, width:] = gc
                va[slot, h, :d] = vt[h * d : (h + 1) * d]

        def scores(slot, u, t):
            h, c = u
            return lax.dot_general(
                ka[slot, h, t * chunk : (t + 1) * chunk],
                qa[h, c * chunk : (c + 1) * chunk],
                (((1,), (1,)), ((), ())),
                preferred_element_type=f32,
            )

        def masked(s, c, t):
            if t < c:
                return s
            kp = lax.broadcasted_iota(jnp.int32, (chunk, chunk), 0)
            qp = lax.broadcasted_iota(jnp.int32, (chunk, chunk), 1)
            return jnp.where(kp <= qp, s, -1e30)

        def step(slot, diagonal, ahead=None):
            count = lambda u: u[1] + 1 if diagonal else chunks
            held = [first[t * chunk : (t + 1) * chunk] for t in range(count(units[0]))]
            if ahead is not None:
                ahead()
            for i, u in enumerate(units):
                h, c = u
                cols = slice(c * chunk, (c + 1) * chunk)
                if diagonal:
                    held = [masked(s, c, t) for t, s in enumerate(held)]
                top = held[0]
                for s in held[1:]:
                    top = jnp.maximum(top, s)
                old = peak[h : h + 1, cols]
                new = jnp.maximum(old, jnp.max(top, axis=0, keepdims=True))
                scaled = new * rate
                factor = jnp.exp2(old * rate - scaled)
                peak[h : h + 1, cols] = new
                following = units[i + 1] if i + 1 < len(units) else None
                coming = []
                total_add = None
                if following:
                    ahead_count = count(following)
                else:
                    ahead_count = 0 if diagonal else chunks
                for t in range(max(len(held), ahead_count)):
                    if t < ahead_count:
                        if following:
                            coming.append(scores(slot, following, t))
                        else:
                            first[t * chunk : (t + 1) * chunk] = scores(1 - slot, units[0], t)
                    if t < len(held):
                        w = jnp.exp2(held[t] * rate - scaled).astype(bf16)
                        add = jnp.dot(va[slot, h, :, t * chunk : (t + 1) * chunk], w, preferred_element_type=f32)
                        total_add = add if total_add is None else total_add + add
                acc[h, :, cols] = acc[h, :, cols] * factor + total_add
                held = coming

        prepare(0, 0)
        for t in range(chunks):
            first[t * chunk : (t + 1) * chunk] = scores(0, units[0], t)

        @pl.loop(0, me)
        def _(j):
            slot = lax.rem(j, 2)
            step(slot, False, lambda: prepare(j + 1, 1 - slot))

        step(lax.rem(me, 2), True)
        outs = [acc[h, :d] / acc[h, d : d + 1] for h in range(heads)]
        o = outs[0] if heads == 1 else jnp.concatenate(outs, axis=0)
        o_ref[...] = o.T.astype(bf16)

    vm = pl.BlockSpec(memory_space=pltpu.VMEM)
    return pl.pallas_call(
        body,
        in_specs=[pl.BlockSpec(memory_space=pltpu.SMEM), vm, vm, vm],
        out_specs=vm,
        scratch_shapes=[
            pltpu.VMEM((heads, rows, deep), bf16),
            pltpu.VMEM((2, heads, rows, deep), bf16),
            pltpu.VMEM((2, heads, ext, rows), bf16),
            pltpu.VMEM((heads, ext, rows), f32),
            pltpu.VMEM((8, rows), f32),
            pltpu.VMEM((rows, chunk), f32),
        ],
        out_shape=jax.ShapeDtypeStruct((rows, width), bf16),
        compiler_params=pltpu.CompilerParams(vmem_limit_bytes=50 * 2**20),
    )(rank, q, kv, gates)


def per_device(
    query_small,
    key_small,
    value_small,
    gates_small,
    query_large,
    key_large,
    value_large,
    gates_large,
    residual,
    mixer_small,
    mixer_large,
    mix_gain,
    value_weight,
    gate_weight,
    value_taps,
    gate_taps,
    down_weight,
    final_gain,
):
    shard_rows = query_small.shape[0]
    rank = lax.axis_index("sp").astype(jnp.int32).reshape(1)
    heads_small = gates_small.shape[1]
    heads_large = gates_large.shape[1]
    own_gates = jnp.concatenate(
        [
            gates_small.T,
            gates_large.T,
            jnp.zeros((8 - heads_small - heads_large, shard_rows), f32),
        ],
        axis=0,
    )
    small_pairs = lax.all_gather(
        jnp.concatenate([key_small, value_small], axis=1), "sp", axis=0, tiled=True
    )
    every_gate = lax.all_gather(own_gates, "sp", axis=0)
    large_pairs = lax.all_gather(
        jnp.concatenate([key_large, value_large], axis=1), "sp", axis=0, tiled=True
    )
    whole_value, whole_gate, whole_down = gather_turned(
        (value_weight, gate_weight, down_weight), "sp", (0, 0, 1)
    )
    small_out = attend(query_small, small_pairs, every_gate, rank, heads_small, 0)
    large_out = attend(query_large, large_pairs, every_gate, rank, heads_large, heads_small)
    tensor_parts = lax.axis_size(TP)
    own_rows = shard_rows // tensor_parts
    joined = jnp.concatenate([small_out, large_out], axis=1)
    pieces = joined.reshape(tensor_parts, own_rows, joined.shape[1])
    arrived = lax.all_to_all(pieces, TP, split_axis=0, concat_axis=0, tiled=True)
    layout = jnp.moveaxis(arrived, 0, 1)
    small_width = small_out.shape[1]
    all_small = layout[:, :, :small_width].reshape(own_rows, tensor_parts * small_width)
    all_large = layout[:, :, small_width:].reshape(own_rows, tensor_parts * large_out.shape[1])
    add_pieces = sent_together((mixer_small, mixer_large), TP, 0, 1)
    mix = jnp.dot(all_small, add_pieces[0], preferred_element_type=jnp.float32) + jnp.dot(
        all_large, add_pieces[1], preferred_element_type=jnp.float32
    )
    mixed = norm_rows(residual_scale * residual.astype(jnp.float32) + mix, mix_gain).astype(
        jnp.bfloat16
    )
    block_input = lax.all_gather(mixed, TP, axis=0, tiled=True)
    up_value = jnp.dot(block_input, whole_value, preferred_element_type=jnp.float32)
    up_gate = jnp.dot(block_input, whole_gate, preferred_element_type=jnp.float32)
    up_value = up_value.astype(jnp.bfloat16)
    up_gate = up_gate.astype(jnp.bfloat16)
    hidden_width = up_value.shape[1]
    trailing = jnp.concatenate([up_value[-2:], up_gate[-2:]], axis=1)
    earlier = passed_along(trailing, "sp", 1)
    padded_value = jnp.concatenate([earlier[:, :hidden_width], up_value], axis=0).astype(
        jnp.float32
    )
    padded_gate = jnp.concatenate([earlier[:, hidden_width:], up_gate], axis=0).astype(jnp.float32)
    filt_value = (
        value_taps[0] * padded_value[:-2]
        + value_taps[1] * padded_value[1:-1]
        + value_taps[2] * padded_value[2:]
    )
    filt_gate = (
        gate_taps[0] * padded_gate[:-2]
        + gate_taps[1] * padded_gate[1:-1]
        + gate_taps[2] * padded_gate[2:]
    )
    hidden = (jax.nn.silu(filt_gate) * filt_value).astype(jnp.bfloat16)
    ffn_terms = jnp.dot(hidden, whole_down, preferred_element_type=jnp.float32)
    ffn = lax.psum_scatter(
        ffn_terms.astype(jnp.bfloat16), TP, scatter_dimension=0, tiled=True
    ).astype(jnp.float32)
    return norm_rows(residual_scale * mixed.astype(jnp.float32) + ffn, final_gain).astype(
        jnp.bfloat16
    )


def solution(mesh):
    split = Mesh(mesh.devices.reshape(mesh.shape["sp"], 4, 2), ("sp", "tp_0", "tp_1"))
    placed = (
        P("sp", TP),
        P("sp", TP),
        P("sp", TP),
        P("sp", TP),
        P("sp", TP),
        P("sp", TP),
        P("sp", TP),
        P("sp", TP),
        P(SP_TP, None),
        P(TP, None),
        P(TP, None),
        P(),
        P("sp", TP),
        P("sp", TP),
        P(None, TP),
        P(None, TP),
        P(TP, "sp"),
        P(),
    )
    return jax.shard_map(
        per_device, mesh=split, in_specs=placed, out_specs=P(SP_TP, None), check_vma=False
    )
```

time: 430 us -> 378 us (0.88)
  blocking collectives: 70.8 us -> 41.1 us
  local copies, waits for them, and re-layouts: 20.1 us -> 1.18 us
  Pallas kernels: 0 us -> 9.03 us
  matrix products: 28.1 us -> 21 us
    all_gather x0 -> x2, waiting for transfers between devices: none -> 93.2 us  [the longest x1 58.4 us: per_device(): lax.all_gather(jnp.concatenate([key_large, value_large], axis=1), 'sp', a...]
    all_gather x1, waiting for transfers between devices: 118 us -> 28.5 us  [per_device(): block_input = lax.all_gather(mixed, TP, axis=0, tiled=True)]
    all_gather x2 -> x1, blocking collectives: 49.1 us -> 26 us  [per_device(): every_gate = lax.all_gather(own_gates, 'sp', axis=0)]
    all_gather x2 -> x1, waiting for transfers between devices: 44.6 us -> 33.1 us  [sent_together(): lax.all_gather(both, axis, axis=dim, tiled=True)]
    pallas_call x0 -> x2, Pallas kernels: none -> 9.03 us  [attend(): pl.pallas_call(body, in_specs=[pl.BlockSpec(memory_space=pltpu.SMEM), vm,...]
    slice x2 -> x0, local copies, waits for them, and re-layouts: 8.68 us -> none  [the longest x1 8.66 us: sent_together(): finished.append(lax.slice_in_dim(out, at, at + a.shape[along], axis=along))]
    unnamed x35, local copies, waits for them, and re-layouts: 8.51 us -> 0.8 us
    dot_general x4 -> x0, matrix products: 7.09 us -> none  [the longest x2 3.91 us: attend_block(): jnp.einsum('hqk,khd->qhd', weights.astype(jnp.bfloat16), value_heads, pre...]
  transfers between devices with their start and end apart: 6 -> 7, of which waited for: 6 -> 7; matrix products, arithmetic and copies ran while one was open for 9% -> 3% of each run, Pallas kernels for 0% -> 2%
where the time goes in v1:
time: 378 us
  waiting for transfers between devices  276 us (73%)
  blocking collectives  41.1 us (11%)
  matrix products  21 us (6%)
  between operations  13.7 us (4%)
  other arithmetic  12.3 us (3%)
  Pallas kernels  9.03 us (2%)
  starting transfers between devices  3.79 us (1%)
    all_gather x1, waiting for transfers between devices, gather_turned(): out = lax.all_gather(both, axis, axis=0, tiled=True)  75.8 us
    all_gather x1, waiting for transfers between devices, per_device(): lax.all_gather(jnp.concatenate([key_large, value_large], axis=1), 'sp', a...  58.4 us
    reduce_scatter x1, waiting for transfers between devices, per_device(): lax.psum_scatter(ffn_terms.astype(jnp.bfloat16), TP, scatter_dimension=0,...  37 us
    all_gather x1, waiting for transfers between devices, per_device(): lax.all_gather(jnp.concatenate([key_small, value_small], axis=1), 'sp', a...  34.9 us
    all_gather x1, waiting for transfers between devices, sent_together(): lax.all_gather(both, axis, axis=dim, tiled=True)  33.1 us
    all_gather x1, waiting for transfers between devices, per_device(): block_input = lax.all_gather(mixed, TP, axis=0, tiled=True)  28.5 us
    all_gather x1, blocking collectives, per_device(): every_gate = lax.all_gather(own_gates, 'sp', axis=0)  26 us
    all_to_all x1, blocking collectives, per_device(): lax.all_to_all(pieces, TP, split_axis=0, concat_axis=0, tiled=True)  15 us
  transfers between devices with their start and end apart: 7, of which 7 were waited for; matrix products, arithmetic and copies ran while one was open for 3% of the time, Pallas kernels for 2%

profile of v1, /device:TPU:0, one launch (start us, length us, event | category | flops | bytes accessed | tf_op | source)
XLA Modules:
  0.0 377.8 jit_solution(4339353494037022348)
XLA Ops:
  6.5 0.0 all-gather.7.cloned.1.call-start
  6.5 1.9 pad_maximum_fusion.2
  8.4 0.0 all-gather.7.cloned.1.call-update
  8.5 0.0 copy-start.5
  8.5 0.0 copy-start.6
  8.5 0.0 copy-start.7
  8.5 0.0 all-gather.9.cloned.1.call-start
  8.6 1.9 pad_maximum_fusion.3
  10.5 0.0 all-gather.9.cloned.1.call-update
  10.5 0.0 copy-start.12
  10.5 0.0 copy-start.13
  10.5 0.0 copy-start
  10.5 0.0 all-gather.11.cloned.1.call-start
  10.6 0.0 copy-done.4
  10.6 0.0 copy-done.3
  10.6 1.1 pad_maximum_fusion
  11.7 0.0 all-gather.11.cloned.1.call-update
  11.8 0.0 all-gather.15.cloned.1.call-start
  11.8 0.0 copy-done.5
  11.8 0.0 copy-done.6
  11.8 0.0 copy-done.7
  11.8 0.8 pad_maximum_fusion.1
  12.7 0.0 all-gather.15.cloned.1.call-update
  12.7 0.0 all-gather.13.cloned.1.call-start
  12.8 0.1 pad.17.clone
  12.8 0.0 copy-done.12
  12.8 0.0 copy-done.13
  12.8 0.1 maximum_maximum_fusion
  12.9 26.0 %all-gather = f32[128,768]{1,0:T(8,128)S(1)} all-gather(f32[8,768]{1,0:T(8,128)S(1)} %maximum_maximum_fusion), channel_id=2, replica_groups=mesh['sp'=16,'tp_0'=4,'tp_1'=2] {'sp'}, dimensions={0}, use_global_device_ids=true | all-gather | bytes 417792 | tf_op jit(solution)/shard_map/all_gather | solution.py:238
  38.9 34.9 %all-gather.7.cloned.1.call-done.kv_ref = bf16[12288,256]{1,0:T(8,128)(2,1)} async-done(((bf16[768,256]{1,0:T(8,128)(2,1)}), bf16[12288,256]{1,0:T(8,128)(2,1)}) %all-gather.7.cloned.1.call-update) | async-done | bytes 6291472 | tf_op jit(solution)/shard_map/all_gather | solution.py:235
  73.8 0.0 copy-done
  73.8 4.8 %shard_map.172 = bf16[768,128]{1,0:T(8,128)(2,1)S(1)} custom-call(s32[1]{0:T(128)} %bitcast.rank_ref, bf16[768,128]{1,0:T(8,128)(2,1)S(1)} %copy-done, bf16[12288,256]{1,0:T(8,128)(2,1)} %all-gather.7.cloned.1.call-done.kv_ref, f32[16,8,768]{2,1,0:T(8,128)S(1)} %bitcast.21), custom_call_target="tpu_custom_call" | custom-call | tf_op jit(solution)/shard_map/pallas_call | solution.py:186
  78.6 58.4 %all-gather.9.cloned.1.call-done.kv_ref = bf16[12288,256]{1,0:T(8,128)(2,1)} async-done(((bf16[768,256]{1,0:T(8,128)(2,1)}), bf16[12288,256]{1,0:T(8,128)(2,1)}) %all-gather.9.cloned.1.call-update) | async-done | bytes 6291472 | tf_op jit(solution)/shard_map/all_gather | solution.py:239
  137.0 4.2 %shard_map.173 = bf16[768,128]{1,0:T(8,128)(2,1)S(1)} custom-call(s32[1]{0:T(128)} %bitcast.rank_ref, bf16[768,128]{1,0:T(8,128)(2,1)S(1)} %copy-done.1, bf16[12288,256]{1,0:T(8,128)(2,1)} %all-gather.9.cloned.1.call-done.kv_ref, f32[16,8,768]{2,1,0:T(8,128)S(1)} %bitcast.22), custom_call_target="tpu_custom_call" | custom-call | tf_op jit(solution)/shard_map/pallas_call | solution.py:186
  141.3 15.0 %all_to_all.5 = bf16[8,96,256]{2,1,0:T(8,128)(2,1)S(1)} all-to-all(bf16[8,96,256]{2,1,0:T(8,128)(2,1)S(1)} %bitcast.24), channel_id=1, replica_groups=mesh['sp'=16,'tp_0'=4,'tp_1'=2] {'tp_0','tp_1'}, dimensions={0} | all-to-all | bytes 786432 | tf_op jit(solution)/shard_map/all_to_all | solution.py:251
  156.3 0.1 slice_bitcast_fusion.1
  156.4 33.1 %all-gather.11.cloned.1.call-done = bf16[1024,4096]{1,0:T(8,128)(2,1)} async-done(((bf16[128,4096]{1,0:T(8,128)(2,1)}), bf16[1024,4096]{1,0:T(8,128)(2,1)}) %all-gather.11.cloned.1.call-update) | async-done | bytes 8388624 | tf_op jit(solution)/shard_map/all_gather | solution.py:39
  189.5 3.0 fusion
  192.5 0.0 copy-start.8
  192.5 3.2 fusion.35
  195.8 0.2 multiply_reduce_fusion.1
  196.0 0.9 multiply_convert_fusion.1
  196.9 0.0 all-gather.13.cloned.1.call-update
  197.0 0.2 reduce-scatter.2.cloned.1.call-start
  197.2 75.8 %all-gather.15.cloned.1.call-done = bf16[2048,2112]{0,1:T(8,128)(2,1)} async-done(((bf16[128,2112]{0,1:T(8,128)(2,1)}), bf16[2048,2112]{0,1:T(8,128)(2,1)}) %all-gather.15.cloned.1.call-update) | async-done | bytes 8650768 | tf_op jit(solution)/shard_map/all_gather | solution.py:27
  273.0 28.5 %all-gather.13.cloned.1.call-done = bf16[768,2048]{1,0:T(8,128)(2,1)} async-done(((bf16[96,2048]{1,0:T(8,128)(2,1)}), bf16[768,2048]{1,0:T(8,128)(2,1)}) %all-gather.13.cloned.1.call-update) | async-done | bytes 3145744 | tf_op jit(solution)/shard_map/all_gather | solution.py:263
  301.5 5.3 %fusion.21 = bf16[768,704]{0,1:T(8,128)(2,1)S(1)} fusion(bf16[768,2048]{1,0:T(8,128)(2,1)} %all-gather.13.cloned.1.call-done, bf16[2048,2112]{0,1:T(8,128)(2,1)} %all-gather.15.cloned.1.call-done), kind=kOutput, calls=%fused_computation.24 | convolution fusion | flops 2215133184 | bytes 7110656 | tf_op jit(solution)/shard_map/dot_general | solution.py:264
  306.9 0.1 slice.84
  307.0 0.7 copy-done.15
  307.7 2.4 fusion.24
  310.1 0.1 slice.85
  310.2 0.1 pad_maximum_fusion.5
  310.3 3.4 collective-permute-start
  313.8 0.1 slice_reduce_fusion.2
  313.8 7.9 %collective-permute-done = bf16[2,1408]{0,1:T(8,128)(2,1)S(1)} collective-permute-done((bf16[2,1408]{0,1:T(8,128)(2,1)S(1)}, bf16[2,1408]{0,1:T(8,128)(2,1)S(1)}, u32[]{:S(2)}, u32[]{:S(2)}) %collective-permute-start) | collective-permute-done | bytes 5664 | tf_op jit(solution)/shard_map/ppermute | solution.py:49
  321.8 1.1 maximum_convert_fusion
  322.9 7.0 %convolution_convert_fusion = bf16[768,2048]{1,0:T(8,128)(2,1)} fusion(bf16[2048,2112]{0,1:T(8,128)(2,1)S(1)} %copy-done.14, f32[770,704]{0,1:T(8,128)S(1)} %get-tuple-element.18, f32[770,704]{0,1:T(8,128)S(1)} %get-tuple-element.17, f32[704]{0:T(1024)S(1)} %get-tuple-element.9, f32[704]{0:T(1024)S(1)} %get-tuple-element.10, f32[704]{0:T(1024)S(1)} %get-tuple-element.8, ...), kind=kOutput, calls=%fused_computation.4 | convolution fusion | flops 2224816128 | bytes 19030016 | tf_op jit(solution)/shard_map/dot_general | solution.py:286
  329.8 0.0 reduce-scatter.2.cloned.1.call-update
  329.9 37.0 %reduce-scatter.2.cloned.1.call-done = bf16[96,2048]{1,0:T(8,128)(2,1)} async-done(((bf16[768,2048]{1,0:T(8,128)(2,1)}), bf16[96,2048]{1,0:T(8,128)(2,1)}) %reduce-scatter.2.cloned.1.call-update) | async-done | bytes 393232 | tf_op jit(solution)/shard_map/reduce_scatter | solution.py:287
  366.9 1.4 fusion.28
  368.3 1.4 multiply_reduce_fusion
  369.7 0.0 copy-done.9
  369.7 0.0 copy-done.2
  369.8 1.2 multiply_convert_fusion
  (23 shorter events, 0.1 us)
Async XLA Ops:
  6.5 4.1 %copy-start.4 = (bf16[128,2048]{1,0:T(8,128)(2,1)S(1)}, bf16[128,2048]{1,0:T(8,128)(2,1)}, u32[]{:S(2)}) copy-start(bf16[128,2048]{1,0:T(8,128)(2,1)} %param.27) | copy-start | bytes 1572868
  6.5 4.1 %copy-start.3 = (bf16[128,2048]{1,0:T(8,128)(2,1)S(1)}, bf16[128,2048]{1,0:T(8,128)(2,1)}, u32[]{:S(2)}) copy-start(bf16[128,2048]{1,0:T(8,128)(2,1)} %param.28) | copy-start | bytes 1572868
  6.5 67.3 %all-gather.7.cloned.1.call-start = ((), (), s32[]{:S(2)}) async-start(), calls=%async_computation.2 | async-start | bytes 6684672 | tf_op jit(solution)/shard_map/all_gather | solution.py:235
  8.5 3.3 copy-start.5
  8.5 3.3 copy-start.6
  8.5 3.3 copy-start.7
  8.5 128.5 %all-gather.9.cloned.1.call-start = ((), (), s32[]{:S(2)}) async-start(), calls=%async_computation.3 | async-start | bytes 6684672 | tf_op jit(solution)/shard_map/all_gather | solution.py:239
  10.5 2.3 copy-start.12
  10.5 2.3 copy-start.13
  10.5 63.3 %copy-start = (bf16[768,128]{1,0:T(8,128)(2,1)S(1)}, bf16[768,128]{1,0:T(8,128)(2,1)}, u32[]{:S(2)}) copy-start(bf16[768,128]{1,0:T(8,128)(2,1)} %q_ref.2) | copy-start | bytes 589828
  10.5 178.9 %all-gather.11.cloned.1.call-start = ((), (), s32[]{:S(2)}) async-start(), calls=%async_computation.4 | async-start | bytes 9437184 | tf_op jit(solution)/shard_map/all_gather | solution.py:39
  11.8 261.2 %all-gather.15.cloned.1.call-start = ((), (), s32[]{:S(2)}) async-start(), calls=%async_computation.6 | async-start | bytes 9191424 | tf_op jit(solution)/shard_map/all_gather | solution.py:27
  12.7 288.8 %all-gather.13.cloned.1.call-start = ((), (), s32[]{:S(2)}) async-start(), calls=%async_computation.5 | async-start | bytes 3538944 | tf_op jit(solution)/shard_map/all_gather | solution.py:263
  73.8 63.2 %copy-start.1 = (bf16[768,128]{1,0:T(8,128)(2,1)S(1)}, bf16[768,128]{1,0:T(8,128)(2,1)}, u32[]{:S(2)}) copy-start(bf16[768,128]{1,0:T(8,128)(2,1)} %q_ref.3) | copy-start | bytes 589828
  189.5 3.0 copy-start.16
  192.5 3.5 copy-start.8
  197.0 169.9 %reduce-scatter.2.cloned.1.call-start = ((), (), s32[]{:S(2)}) async-start(), calls=%async_computation.7 | async-start | bytes 3538944 | tf_op jit(solution)/shard_map/reduce_scatter | solution.py:287
  301.5 5.5 %copy-start.14 = (bf16[2048,2112]{0,1:T(8,128)(2,1)S(1)}, bf16[2048,2112]{0,1:T(8,128)(2,1)}, u32[]{:S(2)}) copy-start(bf16[2048,2112]{0,1:T(8,128)(2,1)} %all-gather.15.cloned.1.call-done) | copy-start | bytes 25952260
  301.5 6.1 %copy-start.15 = (bf16[768,2048]{1,0:T(8,128)(2,1)S(1)}, bf16[768,2048]{1,0:T(8,128)(2,1)}, u32[]{:S(2)}) copy-start(bf16[768,2048]{1,0:T(8,128)(2,1)} %all-gather.13.cloned.1.call-done) | copy-start | bytes 9437188
  307.7 6.1 %copy-start.10 = (f32[3,704]{1,0:T(4,128)S(1)}, f32[3,704]{1,0:T(4,128)}, u32[]{:S(2)}) copy-start(f32[3,704]{1,0:T(4,128)} %param.32) | copy-start | bytes 25348
  307.7 6.1 %copy-start.11 = (f32[3,704]{1,0:T(4,128)S(1)}, f32[3,704]{1,0:T(4,128)}, u32[]{:S(2)}) copy-start(f32[3,704]{1,0:T(4,128)} %param.33) | copy-start | bytes 25348
  310.3 11.4 %collective-permute-start = (bf16[2,1408]{0,1:T(8,128)(2,1)S(1)}, bf16[2,1408]{0,1:T(8,128)(2,1)S(1)}, u32[]{:S(2)}, u32[]{:S(2)}) collective-permute-start(bf16[2,1408]{0,1:T(8,128)(2,1)S(1)} %pad_maximum_fusion.5), channel_id=1, source_target_pairs={{0,8},{8,16},{16,24},{24,32},{32,40},{40,48},{48,56},{56,64},{64,7... | collective-permute-start | bytes 16904 | tf_op jit(solution)/shard_map/ppermute | solution.py:49
  329.8 39.9 %copy-start.9 = (f32[2048]{0:T(1024)S(1)}, f32[2048]{0:T(1024)}, u32[]{:S(2)}) copy-start(f32[2048]{0:T(1024)} %param.35) | copy-start | bytes 24580
  366.9 2.9 copy-start.2
Sparse Core Ops, SparseCore 0:
  9.5 64.3 all-gather.6
  76.0 60.9 all-gather.8
  138.7 50.7 all-gather.10
  191.4 81.5 all-gather.14
  274.5 26.9 all-gather.12
  330.0 36.8 reduce-scatter.1
